TPU v7x, 256 devices: a 4x2x16 block of a 4x16x16 slice. The times are simulated.
256 devices in a mesh: grp: 2 (over y), sp: 16 (over z), tp: 8 (over x, core).
Axes of the slice: x: 4, y: 2, z: 16, core: 2. Of those that a mesh axis runs over, the one named last changes fastest.
The devices are a block of a 4x16x16 slice.
Arguments:
- queries: bfloat16 [24576, 1024], P(('grp', 'sp'), 'tp'), parts along dimension 0, may hold values from -200 to 200
- key_rows: bfloat16 [24576, 512], P(('grp', 'sp'), 'tp'), parts along dimension 0, may hold values from -6 to 6
- value_rows: bfloat16 [24576, 512], P(('grp', 'sp'), 'tp'), parts along dimension 0, may hold values from -6 to 6
- doc_ids: int32 [24576], P(('grp', 'sp')), parts along dimension 0, may hold values from 0 to 7, never falling along the last dimension, each value on 1 to 3072 neighbouring positions
- sink_logits: float32 [16], P('tp'), may hold values from 2 to 7
- out_weight: bfloat16 [1024, 2048], P('tp', 'sp'), may hold values from -0.1875 to 0.1875
- residual: bfloat16 [24576, 2048], P(('grp', 'sp', 'tp')), parts along dimension 0, may hold values from -6 to 6
- gain_mixed: float32 [2048], replicated, may hold values from 0.1 to 1.9
- gain_before: float32 [2048], replicated, may hold values from 0.1 to 1.9
- gain_after: float32 [2048], replicated, may hold values from 0.1 to 1.9
- gate_weight: bfloat16 [2048, 6144], P('sp', 'tp'), may hold values from -0.125 to 0.125
- up_weight: bfloat16 [2048, 6144], P('sp', 'tp'), may hold values from -0.125 to 0.125
- down_weight: bfloat16 [6144, 2048], P('tp', 'sp'), may hold values from -0.078125 to 0.078125
Outputs:
- layer_out: bfloat16 [24576, 2048], P(('grp', 'sp', 'tp')), parts along dimension 0
There are 2 independent parts, one for each index of `grp`. A program takes and returns all parts, laid end to end along the dimension named above; an argument that names none is the same for every part. Nothing has to cross between parts.
All inputs are finite; a program needn't handle non-finite values.
Results may differ from a plain program's by a relative error of at most 0.015.
Values may be sent and summed in bfloat16 or wider, within the bound.
A program may use at most 128 MiB of HBM per device.

v0:
```python
import jax
import jax.numpy as jnp
from jax import lax
from jax.sharding import PartitionSpec as P

HEAD_DIM = 64
WINDOW = 128
epsilon = 1e-06
masked_value = -1e30


def passed_along(value, axis, steps):
    count = lax.axis_size(axis)
    first, last = (max(0, -steps), min(count, count - steps))
    return lax.ppermute(value, axis, [(source, source + steps) for source in range(first, last)])


def from_everyone(shard, axis):
    size = lax.axis_size(axis)
    return lax.all_to_all(
        jnp.broadcast_to(shard[None], (size, *shard.shape)), axis, 0, 0, tiled=True
    )


def laid_out(pieces, dim):
    pieces = jnp.moveaxis(pieces, 0, dim)
    lengths = pieces.shape
    return pieces.reshape(*lengths[:dim], lengths[dim] * lengths[dim + 1], *lengths[dim + 2 :])


def gather_directly(shard, axis, dim):
    pieces = from_everyone(shard, axis)
    return laid_out(pieces, dim)


def turned_gather(arrays, axis, dims):
    turned = [jnp.moveaxis(a, dim, 0) for a, dim in zip(arrays, dims)]
    both = jnp.concatenate([t.reshape(len(t), -1) for t in turned], axis=1)
    filled, at, finished = (lax.all_gather(both, axis, axis=0, tiled=True), 0, [])
    for t, dim in zip(turned, dims):
        piece = filled[:, at : at + t[0].size].reshape(-1, *t.shape[1:])
        finished.append(jnp.moveaxis(piece, 0, dim))
        at += t[0].size
    return tuple(finished)


def split_up(shard, dim, size):
    lengths = shard.shape
    pieces = shard.reshape(*lengths[:dim], size, lengths[dim] // size, *lengths[dim + 1 :])
    return jnp.moveaxis(pieces, dim, 0)


def summed_on_arrival(shard, axis, dim):
    size = lax.axis_size(axis)
    pieces = lax.all_to_all(split_up(shard, dim, size), axis, 0, 0, tiled=True)
    return jnp.sum(pieces.astype(jnp.float32), axis=0)


def stored(value):
    return lax.optimization_barrier(value.astype(jnp.bfloat16)).astype(jnp.float32)


def rms_scaled(value, gain):
    return value * lax.rsqrt(jnp.mean(value * value, axis=-1, keepdims=True) + epsilon) * gain


def windows(array, blocks):
    first = array[:-WINDOW].reshape((blocks, WINDOW) + array.shape[1:])
    second = array[WINDOW:].reshape((blocks, WINDOW) + array.shape[1:])
    return jnp.concatenate([first, second], axis=1)


def attend(queries, key_rows, value_rows, doc_ids, sink_logits):
    length = queries.shape[0]
    blocks = length // WINDOW
    local_kv = key_rows.shape[1] // HEAD_DIM
    group_size = queries.shape[1] // HEAD_DIM // local_kv
    offset = lax.axis_index("sp") * length
    tail_keys, tail_values, tail_docs = passed_along(
        (key_rows[length - WINDOW :], value_rows[length - WINDOW :], doc_ids[length - WINDOW :]),
        "sp",
        1,
    )
    key_blocks = windows(jnp.concatenate([tail_keys, key_rows], axis=0), blocks).reshape(
        blocks, 2 * WINDOW, local_kv, HEAD_DIM
    )
    value_blocks = windows(jnp.concatenate([tail_values, value_rows], axis=0), blocks).reshape(
        blocks, 2 * WINDOW, local_kv, HEAD_DIM
    )
    key_docs = windows(jnp.concatenate([tail_docs, doc_ids], axis=0), blocks)
    key_places = windows(offset - WINDOW + jnp.arange(length + WINDOW, dtype=jnp.int32), blocks)
    query_places = (offset + jnp.arange(length, dtype=jnp.int32)).reshape(blocks, WINDOW)
    query_docs = doc_ids.reshape(blocks, WINDOW)
    query_blocks = queries.reshape(blocks, WINDOW, local_kv, group_size, HEAD_DIM)
    scores = jnp.einsum(
        "bqhgd,bkhd->bhgqk", query_blocks, key_blocks, preferred_element_type=jnp.float32
    ) * HEAD_DIM ** (-0.5)
    distance = query_places[:, :, None] - key_places[:, None, :]
    valid = (distance >= 0) & (distance < WINDOW) & (key_places[:, None, :] >= 0)
    valid = valid & (query_docs[:, :, None] == key_docs[:, None, :])
    scores = jnp.where(valid[:, None, None], scores, masked_value)
    sinks = sink_logits.reshape(local_kv, group_size)[None, :, :, None]
    top = jnp.maximum(jnp.max(scores, axis=-1), sinks)
    weight = jnp.exp(scores - top[..., None])
    denom = jnp.sum(weight, axis=-1) + jnp.exp(sinks - top)
    summed = jnp.einsum(
        "bhgqk,bkhd->bqhgd",
        weight.astype(jnp.bfloat16),
        value_blocks,
        preferred_element_type=jnp.float32,
    )
    scale = jnp.transpose(denom, (0, 3, 1, 2))[..., None]
    return (summed / scale).reshape(length, queries.shape[1]).astype(jnp.bfloat16)


def per_device(
    queries,
    key_rows,
    value_rows,
    doc_ids,
    sink_logits,
    out_weight,
    residual,
    gain_mixed,
    gain_before,
    gain_after,
    gate_weight,
    up_weight,
    down_weight,
):
    mixed = attend(queries, key_rows, value_rows, doc_ids, sink_logits)
    head_columns = gather_directly(out_weight, "sp", 1)
    by_rows = lax.all_to_all(mixed, "tp", split_axis=0, concat_axis=1, tiled=True)
    projected = jnp.dot(
        by_rows,
        lax.all_gather(head_columns, "tp", axis=0, tiled=True),
        preferred_element_type=jnp.float32,
    )
    projected = stored(projected)
    after = stored(residual.astype(jnp.float32) + rms_scaled(projected, gain_mixed))
    normed = rms_scaled(after, gain_before).astype(jnp.bfloat16)
    full_gate, full_up, full_down = turned_gather(
        (gate_weight, up_weight, down_weight), "sp", (0, 0, 1)
    )
    piece = lax.all_gather(normed, "tp", axis=0, tiled=True)
    gate = jnp.dot(piece, full_gate, preferred_element_type=jnp.float32)
    upward = jnp.dot(piece, full_up, preferred_element_type=jnp.float32)
    hidden = (jax.nn.silu(gate) * upward).astype(jnp.bfloat16)
    ffn_out = stored(
        summed_on_arrival(
            jnp.dot(hidden, full_down, preferred_element_type=jnp.float32).astype(jnp.bfloat16),
            "tp",
            0,
        )
    )
    return (after + 0.5 * rms_scaled(ffn_out, gain_after)).astype(jnp.bfloat16)


def solution(mesh):
    return jax.shard_map(
        per_device,
        mesh=mesh,
        in_specs=(
            P(("grp", "sp"), "tp"),
            P(("grp", "sp"), "tp"),
            P(("grp", "sp"), "tp"),
            P(("grp", "sp")),
            P("tp"),
            P("tp", "sp"),
            P(("grp", "sp", "tp"), None),
            P(),
            P(),
            P(),
            P("sp", "tp"),
            P("sp", "tp"),
            P("tp", "sp"),
        ),
        out_specs=P(("grp", "sp", "tp"), None),
        check_vma=False,
    )
```

profile of v0, /device:TPU:33, one launch (start us, length us, event | category | flops | bytes accessed | tf_op | source)
XLA Modules:
  0.0 348.9 jit_solution(4281266326615611289)
XLA Ops:
  6.5 0.0 copy-start.7
  6.5 0.0 copy-start.1
  6.6 0.0 copy-start
  6.6 0.1 all-gather.4.cloned.1.call-start
  6.6 1.0 copy.40
  7.6 0.1 broadcast_in_dim.16
  7.7 47.2 %all_to_all.26 = bf16[16,128,128]{1,2,0:T(8,128)(2,1)} all-to-all(bf16[16,128,128]{1,2,0:T(8,128)(2,1)S(1)} %broadcast_in_dim.16), channel_id=1, replica_groups=mesh['grp'=2,'sp'=16,'tp'=8] {'sp'}, dimensions={0} | all-to-all | bytes 1048576 | tf_op jit(solution)/shard_map/all_to_all | solution.py:20
  54.9 0.1 all-gather.4.cloned.1.call-update
  54.9 0.1 all-gather.6.cloned.1.call-start
  55.0 0.7 slice.49
  55.7 5.3 %collective-permute-start.1 = (s32[128]{0:T(128)S(1)}, s32[128]{0:T(128)S(1)}, u32[]{:S(2)}, u32[]{:S(2)}) collective-permute-start(s32[128]{0:T(128)S(1)} %slice.49), channel_id=1, source_target_pairs={{0,8},{8,16},{16,24},{24,32},{32,40},{40,48},{48,56},{56,64},{64,7... | collective-permute-start | bytes 1544 | tf_op jit(solution)/shard_map/ppermute | solution.py:15
  61.0 0.7 slice.45
  61.7 2.2 collective-permute-start
  63.9 0.7 slice.52
  64.6 4.6 %collective-permute-start.2 = (bf16[128,64]{0,1:T(8,128)(2,1)S(1)}, bf16[128,64]{0,1:T(8,128)(2,1)S(1)}, u32[]{:S(2)}, u32[]{:S(2)}) collective-permute-start(bf16[128,64]{0,1:T(8,128)(2,1)S(1)} %slice.52), channel_id=1, source_target_pairs={{0,8},{8,16},{16,24},{24,32},{32,40},{40,48},{48,56},{56,64},{64,7... | collective-permute-start | bytes 49160 | tf_op jit(solution)/shard_map/ppermute | solution.py:15
  69.2 0.0 copy-done
  69.3 0.0 copy-done.1
  69.3 0.0 copy-done.6
  69.3 0.2 reshape.170
  69.5 0.0 collective-permute-done.1
  69.5 0.0 copy-done.7
  69.6 1.0 fusion.30
  70.6 0.0 collective-permute-done.2
  70.6 0.0 collective-permute-done
  70.6 0.5 fusion.48
  71.1 0.0 copy-done.11
  71.1 0.1 broadcast_maximum_fusion
  71.2 0.2 fusion.7
  71.4 0.1 fusion.43
  71.5 0.4 fusion.13
  71.9 0.4 copy.48
  72.3 0.2 reshape.171
  72.5 17.5 %all_to_all.27 = bf16[8,96,128]{2,1,0:T(8,128)(2,1)S(1)} all-to-all(bf16[8,96,128]{2,1,0:T(8,128)(2,1)S(1)} %reshape.171), channel_id=1, replica_groups=mesh['grp'=2,'sp'=16,'tp'=8] {'tp'}, dimensions={0} | all-to-all | bytes 393216 | tf_op jit(solution)/shard_map/all_to_all | solution.py:133
  90.0 12.1 %all-gather.4.cloned.1.call-done = bf16[1024,2048]{0,1:T(8,128)(2,1)} async-done(((bf16[128,2048]{0,1:T(8,128)(2,1)}), bf16[1024,2048]{0,1:T(8,128)(2,1)}) %all-gather.4.cloned.1.call-update) | async-done | bytes 4194320 | tf_op jit(solution)/shard_map/all_gather | solution.py:136
  102.2 3.6 %convolution_convert_fusion.1 = bf16[96,2048]{1,0:T(8,128)(2,1)S(1)} fusion(bf16[1024,2048]{0,1:T(8,128)(2,1)} %all-gather.4.cloned.1.call-done, bf16[8,96,128]{2,1,0:T(8,128)(2,1)S(1)} %all_to_all.27), kind=kOutput, calls=%fused_computation.7 | convolution fusion | flops 402849792 | bytes 4784128 | tf_op jit(solution)/shard_map/dot_general | solution.py:134
  105.8 0.0 copy-start.4
  105.8 0.0 copy-start.5
  105.8 0.0 copy-start.3
  105.8 0.2 fusion.14
  106.0 0.0 copy-done.2
  106.0 0.0 copy-done.8
  106.0 0.2 fusion.17
  106.2 0.2 fusion.21
  106.4 0.0 copy-done.9
  106.4 0.9 fusion.23
  107.3 0.1 all-gather.6.cloned.1.call-update
  107.4 0.2 all-gather.8.cloned.1.call-start
  107.6 0.0 copy-done.4
  107.6 0.2 copy.41
  107.8 0.0 copy-done.5
  107.8 0.2 copy.42
  108.0 0.0 copy-done.3
  108.0 0.9 pad_maximum_fusion
  108.9 0.1 all-gather.8.cloned.1.call-update
  108.9 31.3 %all-gather.6.cloned.1.call-done = bf16[768,2048]{1,0:T(8,128)(2,1)} async-done(((bf16[96,2048]{1,0:T(8,128)(2,1)}), bf16[768,2048]{1,0:T(8,128)(2,1)}) %all-gather.6.cloned.1.call-update) | async-done | bytes 3145744 | tf_op jit(solution)/shard_map/all_gather | solution.py:145
  140.2 128.3 %all-gather.8.cloned.1.call-done = bf16[2048,2304]{0,1:T(8,128)(2,1)} async-done(((bf16[128,2304]{0,1:T(8,128)(2,1)}), bf16[2048,2304]{0,1:T(8,128)(2,1)}) %all-gather.8.cloned.1.call-update) | async-done | bytes 9437200 | tf_op jit(solution)/shard_map/all_gather | solution.py:39
  268.5 6.9 %fusion.3 = f32[768,768]{1,0:T(8,128)} fusion(bf16[768,2048]{1,0:T(8,128)(2,1)} %all-gather.6.cloned.1.call-done, bf16[2048,2304]{0,1:T(8,128)(2,1)} %all-gather.8.cloned.1.call-done), kind=kOutput, calls=%fused_computation.4 | convolution fusion | flops 2415919104 | bytes 8650752 | tf_op jit(solution)/shard_map/dot_general | solution.py:146
  275.4 0.0 copy-done.12
  275.4 11.0 %convolution_convert_fusion = bf16[768,2048]{1,0:T(8,128)(2,1)} fusion(bf16[2048,2304]{0,1:T(8,128)(2,1)} %all-gather.8.cloned.1.call-done, f32[768,768]{1,0:T(8,128)} %fusion.3, bf16[768,2048]{1,0:T(8,128)(2,1)S(1)} %copy-done.12), kind=kOutput, calls=%fused_computation | convolution fusion | flops 4836950016 | bytes 14942208 | tf_op jit(solution)/shard_map/dot_general | solution.py:151
  286.4 51.4 %all_to_all.28 = bf16[8,96,2048]{2,1,0:T(8,128)(2,1)S(1)} all-to-all(bf16[8,96,2048]{2,1,0:T(8,128)(2,1)} %bitcast.84), channel_id=1, replica_groups=mesh['grp'=2,'sp'=16,'tp'=8] {'tp'}, dimensions={0} | all-to-all | bytes 6291456 | tf_op jit(solution)/shard_map/all_to_all | solution.py:55
  337.7 1.4 reduce_sum.54
  339.2 1.2 fusion.18
  340.3 0.0 copy-done.10
  340.4 2.0 fusion.24
  (21 shorter events, 0.2 us)
Async XLA Ops:
  6.5 63.0 %copy-start.7 = (s32[768]{0:T(1024)S(1)}, s32[768]{0:T(1024)}, u32[]{:S(2)}) copy-start(s32[768]{0:T(1024)} %param.16) | copy-start | bytes 9220
  6.5 62.7 %copy-start.1 = (bf16[768,64]{0,1:T(8,128)(2,1)S(1)}, bf16[768,64]{0,1:T(8,128)(2,1)}, u32[]{:S(2)}) copy-start(bf16[768,64]{0,1:T(8,128)(2,1)} %param.15) | copy-start | bytes 294916
  6.6 62.7 %copy-start = (bf16[768,64]{0,1:T(8,128)(2,1)S(1)}, bf16[768,64]{0,1:T(8,128)(2,1)}, u32[]{:S(2)}) copy-start(bf16[768,64]{0,1:T(8,128)(2,1)} %param.14) | copy-start | bytes 294916
  6.6 62.8 %copy-start.6 = (bf16[768,128]{1,0:T(8,128)(2,1)S(1)}, bf16[768,128]{1,0:T(8,128)(2,1)}, u32[]{:S(2)}) copy-start(bf16[768,128]{1,0:T(8,128)(2,1)} %param.13) | copy-start | bytes 589828
  6.6 95.6 %all-gather.4.cloned.1.call-start = ((), (), s32[]{:S(2)}) async-start(), calls=%async_computation.3 | async-start | bytes 4718592 | tf_op jit(solution)/shard_map/all_gather | solution.py:136
  54.9 16.2 %copy-start.11 = (f32[2]{0:T(128)S(1)}, f32[2]{0:T(128)}, u32[]{:S(2)}) copy-start(f32[2]{0:T(128)} %param.17) | copy-start | bytes 28
  54.9 85.2 %all-gather.6.cloned.1.call-start = ((), (), s32[]{:S(2)}) async-start(), calls=%async_computation.4 | async-start | bytes 3538944 | tf_op jit(solution)/shard_map/all_gather | solution.py:145
  55.7 13.8 %collective-permute-start.1 = (s32[128]{0:T(128)S(1)}, s32[128]{0:T(128)S(1)}, u32[]{:S(2)}, u32[]{:S(2)}) collective-permute-start(s32[128]{0:T(128)S(1)} %slice.49), channel_id=1, source_target_pairs={{0,8},{8,16},{16,24},{24,32},{32,40},{40,48},{48,56},{56,64},{64,7... | collective-permute-start | bytes 1544 | tf_op jit(solution)/shard_map/ppermute | solution.py:15
  61.7 8.9 %collective-permute-start = (bf16[128,64]{0,1:T(8,128)(2,1)S(1)}, bf16[128,64]{0,1:T(8,128)(2,1)S(1)}, u32[]{:S(2)}, u32[]{:S(2)}) collective-permute-start(bf16[128,64]{0,1:T(8,128)(2,1)S(1)} %slice.45), channel_id=1, source_target_pairs={{0,8},{8,16},{16,24},{24,32},{32,40},{40,48},{48,56},{56,64},{64,7... | collective-permute-start | bytes 49160 | tf_op jit(solution)/shard_map/ppermute | solution.py:15
  64.6 5.9 %collective-permute-start.2 = (bf16[128,64]{0,1:T(8,128)(2,1)S(1)}, bf16[128,64]{0,1:T(8,128)(2,1)S(1)}, u32[]{:S(2)}, u32[]{:S(2)}) collective-permute-start(bf16[128,64]{0,1:T(8,128)(2,1)S(1)} %slice.52), channel_id=1, source_target_pairs={{0,8},{8,16},{16,24},{24,32},{32,40},{40,48},{48,56},{56,64},{64,7... | collective-permute-start | bytes 49160 | tf_op jit(solution)/shard_map/ppermute | solution.py:15
  90.0 16.0 %copy-start.2 = (bf16[96,2048]{1,0:T(8,128)(2,1)S(1)}, bf16[96,2048]{1,0:T(8,128)(2,1)}, u32[]{:S(2)}) copy-start(bf16[96,2048]{1,0:T(8,128)(2,1)} %param.19) | copy-start | bytes 1179652
  90.0 16.0 %copy-start.8 = (f32[2048]{0:T(1024)S(1)}, f32[2048]{0:T(1024)}, u32[]{:S(2)}) copy-start(f32[2048]{0:T(1024)} %param.20) | copy-start | bytes 24580
  90.0 16.4 %copy-start.9 = (f32[2048]{0:T(1024)S(1)}, f32[2048]{0:T(1024)}, u32[]{:S(2)}) copy-start(f32[2048]{0:T(1024)} %param.21) | copy-start | bytes 24580
  105.8 1.9 copy-start.4
  105.8 2.0 copy-start.5
  105.8 2.2 copy-start.3
  107.4 161.1 %all-gather.8.cloned.1.call-start = ((), (), s32[]{:S(2)}) async-start(), calls=%async_computation.5 | async-start | bytes 10027008 | tf_op jit(solution)/shard_map/all_gather | solution.py:39
  140.2 135.2 %copy-start.12 = (bf16[768,2048]{1,0:T(8,128)(2,1)S(1)}, bf16[768,2048]{1,0:T(8,128)(2,1)}, u32[]{:S(2)}) copy-start(bf16[768,2048]{1,0:T(8,128)(2,1)} %all-gather.6.cloned.1.call-done) | copy-start | bytes 9437188
  337.7 2.6 copy-start.10
Sparse Core Ops, SparseCore 0:
  55.1 47.0 all-gather.3
  107.5 32.6 all-gather.5
  141.9 126.5 all-gather.7
where the time goes:
time: 349 us
  waiting for transfers between devices  172 us (49%)
  blocking collectives  116 us (33%)
  matrix products  22.3 us (6%)
  between operations  13.5 us (4%)
  starting transfers between devices  12.4 us (4%)
  other arithmetic  8.34 us (2%)
  local copies, waits for them, and re-layouts  4.39 us (1%)
    all_gather x1, waiting for transfers between devices, turned_gather(): lax.all_gather(both, axis, axis=0, tiled=True)  128 us
    all_to_all x1, blocking collectives, summed_on_arrival(): pieces = lax.all_to_all(split_up(shard, dim, size), axis, 0, 0, tiled=True)  51.4 us
    all_to_all x1, blocking collectives, from_everyone(): lax.all_to_all(jnp.broadcast_to(shard[None], (size, *shard.shape)), axis,...  47.2 us
    all_gather x1, waiting for transfers between devices, per_device(): piece = lax.all_gather(normed, 'tp', axis=0, tiled=True)  31.3 us
    all_to_all x1, blocking collectives, per_device(): lax.all_to_all(mixed, 'tp', split_axis=0, concat_axis=1, tiled=True)  17.5 us
    all_gather x1, waiting for transfers between devices, per_device(): lax.all_gather(head_columns, 'tp', axis=0, tiled=True)  12.1 us
    ppermute x3, starting transfers between devices, passed_along(): lax.ppermute(value, axis, [(source, source + steps) for source in range(f...  12 us
    dot_general x1, matrix products, per_device(): jnp.dot(hidden, full_down, preferred_element_type=jnp.float32)  11 us
  transfers between devices with their start and end apart: 6, of which 3 were waited for; matrix products, arithmetic and copies ran while one was open for 2% of the time, Pallas kernels for 0%

commit v1 on v0

--- a/solution.py
+++ b/solution.py
@@ -36,7 +36,13 @@
 def turned_gather(arrays, axis, dims):
     turned = [jnp.moveaxis(a, dim, 0) for a, dim in zip(arrays, dims)]
     both = jnp.concatenate([t.reshape(len(t), -1) for t in turned], axis=1)
-    filled, at, finished = (lax.all_gather(both, axis, axis=0, tiled=True), 0, [])
+    filled, at, finished = (
+        jnp.concatenate(
+            lax.all_to_all(jnp.stack([both] * lax.axis_size(axis)), axis, 0, 0), axis=0
+        ),
+        0,
+        [],
+    )
     for t, dim in zip(turned, dims):
         piece = filled[:, at : at + t[0].size].reshape(-1, *t.shape[1:])
         finished.append(jnp.moveaxis(piece, 0, dim))

time: 349 us -> 585 us (1.68)
  waiting for transfers between devices: 172 us -> 429 us
  blocking collectives: 116 us -> 42.4 us
  starting transfers between devices: 12.4 us -> 53.1 us
  local copies, waits for them, and re-layouts: 4.39 us -> 12.6 us
    all_to_all x0 -> x3, waiting for transfers between devices: none -> 349 us  [the longest x1 321 us: turned_gather(): lax.all_to_all(jnp.stack([both] * lax.axis_size(axis)), axis, 0, 0)]
    all_gather x1 -> x0, waiting for transfers between devices: 128 us -> none  [turned_gather(): lax.all_gather(both, axis, axis=0, tiled=True)]
    all_to_all x2 -> x0, blocking collectives: 64.7 us -> none  [the longest x1 47.2 us: from_everyone(): lax.all_to_all(jnp.broadcast_to(shard[None], (size, *shard.shape)), axis,...]
    all_to_all x0 -> x3, starting transfers between devices: none -> 38.7 us  [the longest x1 13.5 us: per_device(): lax.all_to_all(mixed, 'tp', split_axis=0, concat_axis=1, tiled=True)]
    all_gather x1, waiting for transfers between devices: 12.1 us -> 44 us  [per_device(): lax.all_gather(head_columns, 'tp', axis=0, tiled=True)]
    all_to_all x1, blocking collectives: 51.4 us -> 42.4 us  [summed_on_arrival(): pieces = lax.all_to_all(split_up(shard, dim, size), axis, 0, 0, tiled=True)]
  transfers between devices with their start and end apart: 6 -> 8, of which waited for: 3 -> 5; matrix products, arithmetic and copies ran while one was open for 2% -> 3% of each run, Pallas kernels for 0% -> 0%
where the time goes in v1:
time: 585 us; the launch traced here: 584 us
  waiting for transfers between devices  429 us (73%)
  starting transfers between devices  53.1 us (9%)
  blocking collectives  42.4 us (7%)
  matrix products  22.4 us (4%)
  between operations  13.8 us (2%)
  local copies, waits for them, and re-layouts  12.6 us (2%)
  other arithmetic  10.5 us (2%)
    all_to_all x1, waiting for transfers between devices, turned_gather(): lax.all_to_all(jnp.stack([both] * lax.axis_size(axis)), axis, 0, 0)  321 us
    all_gather x1, waiting for transfers between devices, per_device(): lax.all_gather(head_columns, 'tp', axis=0, tiled=True)  44 us
    all_to_all x1, blocking collectives, summed_on_arrival(): pieces = lax.all_to_all(split_up(shard, dim, size), axis, 0, 0, tiled=True)  42.4 us
    all_gather x1, waiting for transfers between devices, per_device(): piece = lax.all_gather(normed, 'tp', axis=0, tiled=True)  34.9 us
    all_to_all x1, waiting for transfers between devices, from_everyone(): lax.all_to_all(jnp.broadcast_to(shard[None], (size, *shard.shape)), axis,...  22.2 us
    ppermute x3, starting transfers between devices, passed_along(): lax.ppermute(value, axis, [(source, source + steps) for source in range(f...  14.1 us
    all_to_all x1, starting transfers between devices, per_device(): lax.all_to_all(mixed, 'tp', split_axis=0, concat_axis=1, tiled=True)  13.5 us
    all_to_all x1, starting transfers between devices, from_everyone(): lax.all_to_all(jnp.broadcast_to(shard[None], (size, *shard.shape)), axis,...  13 us
  transfers between devices with their start and end apart: 8, of which 5 were waited for; matrix products, arithmetic and copies ran while one was open for 3% of the time, Pallas kernels for 0%

profile of v1, /device:TPU:33, one launch (start us, length us, event | category | flops | bytes accessed | tf_op | source)
XLA Modules:
  0.0 583.7 jit_solution(6348786215243899382)
XLA Ops:
  6.5 0.7 slice.52
  7.3 5.2 collective-permute-start.2
  12.5 0.7 slice.49
  13.2 4.4 collective-permute-start.1
  17.7 0.7 slice.45
  18.4 4.4 collective-permute-start
  22.8 0.9 copy_bitcast_fusion
  23.7 0.9 copy_bitcast_fusion.2
  24.7 1.1 reshape.176
  25.8 0.0 copy-start.1
  25.8 0.0 collective-permute-done.1
  25.8 0.7 pad_add_fusion.2
  26.6 0.7 pad_add_fusion
  27.3 1.7 fusion.30
  28.9 0.0 collective-permute-done.2
  29.0 0.9 copy_bitcast_fusion.1
  29.9 0.5 fusion.48
  30.3 0.0 copy-done.10
  30.3 0.1 broadcast_maximum_fusion
  30.4 0.2 fusion.7
  30.6 0.0 copy-start.6
  30.7 0.1 fusion.43
  30.7 0.0 collective-permute-done
  30.8 0.0 copy-done.1
  30.8 0.0 copy-start.4
  30.8 0.4 fusion.13
  31.2 0.0 copy-start.5
  31.2 0.0 copy-start.3
  31.2 0.4 copy.51
  31.6 0.9 reshape.177
  32.5 13.5 %all-to-all-start = ((bf16[8,96,128]{2,1,0:T(8,128)(2,1)}), bf16[8,96,128]{2,1,0:T(8,128)(2,1)S(1)}, u32[]{:S(2)}, u32[]{:S(2)}) async-start(bf16[8,96,128]{2,1,0:T(8,128)(2,1)} %reshape.177), calls=%async_computation | async-start | bytes 393216 | tf_op jit(solution)/shard_map/all_to_all | solution.py:139
  46.0 0.1 copy.42
  46.1 5.8 all-to-all-done
  51.9 0.9 broadcast_in_dim.16
  52.8 13.0 %all-to-all-start.1 = ((bf16[16,128,128]{1,2,0:T(8,128)(2,1)}), bf16[16,128,128]{1,2,0:T(8,128)(2,1)S(1)}, u32[]{:S(2)}, u32[]{:S(2)}) async-start(bf16[16,128,128]{1,2,0:T(8,128)(2,1)} %broadcast_in_dim.16), calls=%async_computation.1 | async-start | bytes 1048576 | tf_op jit(solution)/shard_map/all_to_all | solution.py:20
  65.8 0.0 copy-done.4
  65.8 0.2 copy.44
  66.0 0.2 copy.43
  66.2 0.2 copy.45
  66.5 22.2 %all-to-all-done.1 = bf16[16,128,128]{1,2,0:T(8,128)(2,1)S(1)} async-done(((bf16[16,128,128]{1,2,0:T(8,128)(2,1)}), bf16[16,128,128]{1,2,0:T(8,128)(2,1)S(1)}, u32[]{:S(2)}, u32[]{:S(2)}) %all-to-all-start.1) | async-done | bytes 524320 | tf_op jit(solution)/shard_map/all_to_all | solution.py:20
  88.7 4.6 stack.2
  93.2 0.0 copy-done
  93.3 12.2 %all-to-all-start.2 = ((bf16[16,128,2304]{2,1,0:T(8,128)(2,1)}), bf16[16,128,2304]{2,1,0:T(8,128)(2,1)}, u32[]{:S(2)}, u32[]{:S(2)}) async-start(bf16[16,128,2304]{2,1,0:T(8,128)(2,1)} %stack.2), calls=%async_computation.2 | async-start | bytes 18874368 | tf_op jit(solution)/shard_map/all_to_all | solution.py:41
  105.5 0.1 all-gather.3.cloned.1.call-start
  105.5 0.7 all-gather.3.cloned.1.call-update
  106.3 0.0 copy-start.2
  106.3 0.0 copy-start.7
  106.3 0.0 copy-start.8
  106.3 0.2 all-gather.5.cloned.1.call-start
  106.6 44.0 %all-gather.3.cloned.1.call-done = bf16[1024,2048]{0,1:T(8,128)(2,1)} async-done(((bf16[128,2048]{0,1:T(8,128)(2,1)}), bf16[1024,2048]{0,1:T(8,128)(2,1)}) %all-gather.3.cloned.1.call-update) | async-done | bytes 4194320 | tf_op jit(solution)/shard_map/all_gather | solution.py:142
  150.6 3.6 convolution_convert_fusion.1
  154.2 0.2 fusion.14
  154.4 0.2 fusion.17
  154.6 0.2 fusion.21
  154.8 0.9 fusion.23
  155.7 0.1 all-gather.5.cloned.1.call-update
  155.7 34.9 %all-gather.5.cloned.1.call-done = bf16[768,2048]{1,0:T(8,128)(2,1)} async-done(((bf16[96,2048]{1,0:T(8,128)(2,1)}), bf16[768,2048]{1,0:T(8,128)(2,1)}) %all-gather.5.cloned.1.call-update) | async-done | bytes 3145744 | tf_op jit(solution)/shard_map/all_gather | solution.py:151
  190.6 321.3 %all-to-all-done.2 = bf16[16,128,2304]{2,1,0:T(8,128)(2,1)} async-done(((bf16[16,128,2304]{2,1,0:T(8,128)(2,1)}), bf16[16,128,2304]{2,1,0:T(8,128)(2,1)}, u32[]{:S(2)}, u32[]{:S(2)}) %all-to-all-start.2) | async-done | bytes 9437216 | tf_op jit(solution)/shard_map/all_to_all | solution.py:41
  511.9 7.0 %fusion.3 = f32[768,768]{1,0:T(8,128)} fusion(bf16[768,2048]{1,0:T(8,128)(2,1)} %all-gather.5.cloned.1.call-done, bf16[2048,2304]{1,0:T(8,128)(2,1)} %bitcast.19), kind=kOutput, calls=%fused_computation.4 | convolution fusion | flops 2415919104 | bytes 8650752 | tf_op jit(solution)/shard_map/dot_general | solution.py:152
  518.8 11.0 %convolution_convert_fusion = bf16[768,2048]{1,0:T(8,128)(2,1)} fusion(bf16[2048,2304]{1,0:T(8,128)(2,1)} %bitcast.19, f32[768,768]{1,0:T(8,128)} %fusion.3, bf16[768,2048]{1,0:T(8,128)(2,1)S(1)} %copy-done.11), kind=kOutput, calls=%fused_computation | convolution fusion | flops 4836950016 | bytes 14942208 | tf_op jit(solution)/shard_map/dot_general | solution.py:157
  529.8 42.4 %all_to_all.31 = bf16[8,96,2048]{2,1,0:T(8,128)(2,1)S(1)} all-to-all(bf16[8,96,2048]{2,1,0:T(8,128)(2,1)} %bitcast.85), channel_id=1, replica_groups=mesh['grp'=2,'sp'=16,'tp'=8] {'tp'}, dimensions={0} | all-to-all | bytes 6291456 | tf_op jit(solution)/shard_map/all_to_all | solution.py:61
  572.2 1.4 reduce_sum.54
  573.6 1.2 fusion.18
  574.8 2.0 fusion.24
  (22 shorter events, 0.1 us)
Async XLA Ops:
  6.5 23.8 %copy-start.10 = (f32[2]{0:T(128)S(1)}, f32[2]{0:T(128)}, u32[]{:S(2)}) copy-start(f32[2]{0:T(128)} %param.17) | copy-start | bytes 28
  7.3 21.7 %collective-permute-start.2 = (bf16[128,64]{0,1:T(8,128)(2,1)S(1)}, bf16[128,64]{0,1:T(8,128)(2,1)S(1)}, u32[]{:S(2)}, u32[]{:S(2)}) collective-permute-start(bf16[128,64]{0,1:T(8,128)(2,1)S(1)} %slice.52), channel_id=1, source_target_pairs={{0,8},{8,16},{16,24},{24,32},{32,40},{40,48},{48,56},{56,64},{64,7... | collective-permute-start | bytes 49160 | tf_op jit(solution)/shard_map/ppermute | solution.py:15
  13.2 12.6 %collective-permute-start.1 = (s32[128]{0:T(128)S(1)}, s32[128]{0:T(128)S(1)}, u32[]{:S(2)}, u32[]{:S(2)}) collective-permute-start(s32[128]{0:T(128)S(1)} %slice.49), channel_id=1, source_target_pairs={{0,8},{8,16},{16,24},{24,32},{32,40},{40,48},{48,56},{56,64},{64,7... | collective-permute-start | bytes 1544 | tf_op jit(solution)/shard_map/ppermute | solution.py:15
  18.4 12.4 %collective-permute-start = (bf16[128,64]{0,1:T(8,128)(2,1)S(1)}, bf16[128,64]{0,1:T(8,128)(2,1)S(1)}, u32[]{:S(2)}, u32[]{:S(2)}) collective-permute-start(bf16[128,64]{0,1:T(8,128)(2,1)S(1)} %slice.45), channel_id=1, source_target_pairs={{0,8},{8,16},{16,24},{24,32},{32,40},{40,48},{48,56},{56,64},{64,7... | collective-permute-start | bytes 49160 | tf_op jit(solution)/shard_map/ppermute | solution.py:15
  25.8 4.9 copy-start.1
  30.6 15.4 %copy-start.6 = (bf16[128,128]{1,0:T(8,128)(2,1)S(1)}, bf16[128,128]{1,0:T(8,128)(2,1)}, u32[]{:S(2)}) copy-start(bf16[128,128]{1,0:T(8,128)(2,1)} %param.18) | copy-start | bytes 98308
  30.8 35.1 %copy-start.4 = (bf16[128,768]{1,0:T(8,128)(2,1)S(1)}, bf16[128,768]{1,0:T(8,128)(2,1)}, u32[]{:S(2)}) copy-start(bf16[128,768]{1,0:T(8,128)(2,1)} %param.24) | copy-start | bytes 589828
  31.2 34.8 %copy-start.5 = (bf16[128,768]{1,0:T(8,128)(2,1)S(1)}, bf16[128,768]{1,0:T(8,128)(2,1)}, u32[]{:S(2)}) copy-start(bf16[128,768]{1,0:T(8,128)(2,1)} %param.23) | copy-start | bytes 589828
  31.2 35.0 %copy-start.3 = (bf16[768,128]{1,0:T(8,128)(2,1)S(1)}, bf16[768,128]{1,0:T(8,128)(2,1)}, u32[]{:S(2)}) copy-start(bf16[768,128]{1,0:T(8,128)(2,1)} %param.25) | copy-start | bytes 589828
  32.5 19.4 %all-to-all-start = ((bf16[8,96,128]{2,1,0:T(8,128)(2,1)}), bf16[8,96,128]{2,1,0:T(8,128)(2,1)S(1)}, u32[]{:S(2)}, u32[]{:S(2)}) async-start(bf16[8,96,128]{2,1,0:T(8,128)(2,1)} %reshape.177), calls=%async_computation | async-start | bytes 393216 | tf_op jit(solution)/shard_map/all_to_all | solution.py:139
  52.8 35.9 %all-to-all-start.1 = ((bf16[16,128,128]{1,2,0:T(8,128)(2,1)}), bf16[16,128,128]{1,2,0:T(8,128)(2,1)S(1)}, u32[]{:S(2)}, u32[]{:S(2)}) async-start(bf16[16,128,128]{1,2,0:T(8,128)(2,1)} %broadcast_in_dim.16), calls=%async_computation.1 | async-start | bytes 1048576 | tf_op jit(solution)/shard_map/all_to_all | solution.py:20
  88.7 4.6 copy-start
  93.3 418.6 %all-to-all-start.2 = ((bf16[16,128,2304]{2,1,0:T(8,128)(2,1)}), bf16[16,128,2304]{2,1,0:T(8,128)(2,1)}, u32[]{:S(2)}, u32[]{:S(2)}) async-start(bf16[16,128,2304]{2,1,0:T(8,128)(2,1)} %stack.2), calls=%async_computation.2 | async-start | bytes 18874368 | tf_op jit(solution)/shard_map/all_to_all | solution.py:41
  105.5 45.1 %all-gather.3.cloned.1.call-start = ((), (), s32[]{:S(2)}) async-start(), calls=%async_computation.4 | async-start | bytes 4718592 | tf_op jit(solution)/shard_map/all_gather | solution.py:142
  106.3 48.1 %copy-start.2 = (bf16[96,2048]{1,0:T(8,128)(2,1)S(1)}, bf16[96,2048]{1,0:T(8,128)(2,1)}, u32[]{:S(2)}) copy-start(bf16[96,2048]{1,0:T(8,128)(2,1)} %param.19) | copy-start | bytes 1179652
  106.3 48.1 %copy-start.7 = (f32[2048]{0:T(1024)S(1)}, f32[2048]{0:T(1024)}, u32[]{:S(2)}) copy-start(f32[2048]{0:T(1024)} %param.20) | copy-start | bytes 24580
  106.3 48.5 %copy-start.8 = (f32[2048]{0:T(1024)S(1)}, f32[2048]{0:T(1024)}, u32[]{:S(2)}) copy-start(f32[2048]{0:T(1024)} %param.21) | copy-start | bytes 24580
  106.3 84.3 %all-gather.5.cloned.1.call-start = ((), (), s32[]{:S(2)}) async-start(), calls=%async_computation.5 | async-start | bytes 3538944 | tf_op jit(solution)/shard_map/all_gather | solution.py:151
  511.9 7.0 %copy-start.11 = (bf16[768,2048]{1,0:T(8,128)(2,1)S(1)}, bf16[768,2048]{1,0:T(8,128)(2,1)}, u32[]{:S(2)}) copy-start(bf16[768,2048]{1,0:T(8,128)(2,1)} %all-gather.5.cloned.1.call-done) | copy-start | bytes 9437188
  572.2 2.6 copy-start.9
Sparse Core Ops, SparseCore 0:
  108.1 42.3 all-gather.2
  155.9 34.7 all-gather.4
